TPU v7x, 512 devices: a whole 4x8x8 slice. The times are simulated.
512 devices in a mesh: sp: 64 (over z, y), fs: 4 (over x), tp: 2 (over core).
Axes of the slice: x: 4, y: 8, z: 8, core: 2. Of those that a mesh axis runs over, the one named last changes fastest.
Arguments:
- tokens: bfloat16 [4, 8192, 2048], P('fs', ('sp', 'tp')), may hold values from -6 to 6
- norm_gain: float32 [2048], replicated, may hold values from 0.1 to 1.9
- gla_query_weight: bfloat16 [2048, 512], P('sp', 'tp'), may hold values from -0.125 to 0.125
- gla_key_weight: bfloat16 [2048, 512], P('sp', 'tp'), may hold values from -0.125 to 0.125
- gla_value_weight: bfloat16 [2048, 1024], P('sp', 'tp'), may hold values from -0.125 to 0.125
- decay_down: bfloat16 [2048, 32], P('sp'), may hold values from -0.125 to 0.125
- decay_up: bfloat16 [32, 512], P(None, 'tp'), may hold values from -1 to 1
- decay_bias: float32 [512], P('tp'), may hold values from 0.5 to 12
- head_gain: float32 [128], replicated, may hold values from 0.1 to 1.9
- window_query_weight: bfloat16 [2048, 1024], P('sp', 'tp'), may hold values from -3 to 3
- window_key_weight: bfloat16 [2048, 256], P('sp', 'tp'), may hold values from -3 to 3
- window_value_weight: bfloat16 [2048, 256], P('sp', 'tp'), may hold values from -0.125 to 0.125
- sink_logit: float32 [16], P('tp'), may hold values from 3 to 7
- gla_output_weight: bfloat16 [1024, 2048], P('tp', 'sp'), may hold values from -0.125 to 0.125
- window_output_weight: bfloat16 [1024, 2048], P('tp', 'sp'), may hold values from -0.125 to 0.125
Outputs:
- mixed: bfloat16 [4, 8192, 2048], P('fs', ('sp', 'tp'))
All inputs are finite; a program needn't handle non-finite values.
Results may differ from a plain program's by a relative error of at most 0.013.
Values may be sent and summed in bfloat16 or wider, within the bound.
A program may use at most 64 MiB of HBM per device.

v0:
```python
import jax
import jax.numpy as jnp
from jax import lax
from jax.sharding import Mesh
from jax.sharding import PartitionSpec as P

KEY_DIM = 64
VALUE_DIM = 128
HEAD_DIM = 64
WINDOW = 128
SPAN = 64
SP = ("sp_0", "sp_1")
SP_TP = ("sp_0", "sp_1", "tp")
GROUP = ("fs", "tp")
EPS = 1e-06
SOFTMAX_TEMPER = 16.0
HIGH = lax.Precision.HIGHEST


def rms_rows(values, gain):
    mean_square = jnp.mean(values * values, axis=-1, keepdims=True)
    return values * lax.rsqrt(mean_square + EPS) * gain


def own_part(value, at, size, dim):
    return lax.dynamic_slice_in_dim(value, at * size, size, axis=dim)


def combine(earlier, later):
    return (later[1][..., None] * earlier[0] + later[0], earlier[1] * later[1])


def carried_in(value):
    start = (jnp.zeros_like(value[0]), jnp.ones_like(value[1]))
    before, subtotal = (start, value)
    for axis in ("sp_1", "sp_0"):
        peers, place = (lax.axis_size(axis), lax.axis_index(axis))
        both = jnp.concatenate(
            [subtotal[0], jnp.broadcast_to(subtotal[1][..., None], subtotal[0].shape[:-1] + (1,))],
            -1,
        )
        pieces = lax.all_gather(both, axis)
        inside, subtotal = (start, start)
        for k in range(peers):
            subtotal = combine(subtotal, (pieces[k, ..., :-1], pieces[k, ..., -1]))
            inside = jax.tree.map(lambda n, o: jnp.where(k < place, n, o), subtotal, inside)
        before = combine(inside, before)
    return before[0]


def per_device(
    tokens,
    norm_gain,
    gla_query_weight,
    gla_key_weight,
    gla_value_weight,
    decay_down,
    decay_up,
    decay_bias,
    head_gain,
    window_query_weight,
    window_key_weight,
    window_value_weight,
    sink_logit,
    gla_output_weight,
    window_output_weight,
):
    x = lax.axis_index("fs")
    rows = lax.all_gather(tokens[0], GROUP, axis=0, tiled=True)
    w_in = jnp.concatenate(
        [
            own_part(gla_query_weight, x, 64, 1),
            own_part(gla_key_weight, x, 64, 1),
            own_part(gla_value_weight, x, 128, 1),
            own_part(window_query_weight, x, 128, 1),
            own_part(window_key_weight, x // 2, 64, 1),
            own_part(window_value_weight, x // 2, 64, 1),
            decay_down,
        ],
        axis=1,
    )
    w_in = lax.all_gather(w_in, SP, axis=0, tiled=True)
    w_out = jnp.concatenate(
        [own_part(gla_output_weight, x, 128, 0), own_part(window_output_weight, x, 128, 0)], axis=0
    ).T
    w_out = lax.all_gather(w_out, SP, axis=0, tiled=True)
    normed = rms_rows(rows.astype(jnp.float32), norm_gain).astype(jnp.bfloat16)
    proj = jnp.dot(normed, w_in, preferred_element_type=jnp.float32).astype(jnp.bfloat16)
    seqs = 4
    spans = rows.shape[0] // seqs // SPAN
    gate = jnp.dot(proj[:, 512:], own_part(decay_up, x, 64, 1), preferred_element_type=jnp.float32)
    log_rate = jax.nn.log_sigmoid(gate + own_part(decay_bias, x, 64, 0)) / SOFTMAX_TEMPER

    def blocks(v):
        return v.astype(jnp.float32).reshape(seqs, spans, SPAN, -1)

    q, k, v = (
        blocks(proj[:, :64]) * KEY_DIM ** (-0.5),
        blocks(proj[:, 64:128]),
        blocks(proj[:, 128:256]),
    )
    within = jnp.cumsum(blocks(log_rate), axis=2)
    block_total = within[:, :, -1]
    q_dec = q * jnp.exp(within)
    k_dec = k * jnp.exp(-within)
    k_end = k * jnp.exp(block_total[:, :, None] - within)
    scores = jnp.einsum("snid,snjd->snij", q_dec, k_dec, precision=HIGH)
    scores = jnp.where(jnp.tril(jnp.ones((SPAN, SPAN), bool)), scores, 0.0)
    local_out = jnp.einsum("snij,snje->snie", scores, v, precision=HIGH)
    update = jnp.einsum("snjd,snje->snde", k_end, v, precision=HIGH)
    decay = jnp.exp(block_total)
    last_state = decay[:, 1, :, None] * update[:, 0] + update[:, 1]
    incoming = carried_in((last_state, decay[:, 0] * decay[:, 1]))
    entering = jnp.stack([incoming, decay[:, 0, :, None] * incoming + update[:, 0]], axis=1)
    wq = proj[:, 256:384].reshape(seqs, WINDOW, 2, HEAD_DIM)
    wkv = proj[:, 384:512].reshape(seqs, WINDOW, 2 * HEAD_DIM)
    ny, nz = (lax.axis_size("sp_1"), lax.axis_size("sp_0"))
    n = ny * nz
    edge = lax.ppermute(wkv, SP, [(i, i + 1) for i in range(n - 1)])
    band = jnp.concatenate([edge, wkv], axis=1)
    s = jnp.einsum("sqhd,skd->shqk", wq, band[..., :64], preferred_element_type=jnp.float32)
    s = s * HEAD_DIM ** (-0.5)
    dist = jnp.arange(WINDOW)[:, None] + WINDOW - jnp.arange(2 * WINDOW)[None]
    ok = (dist >= 0) & (dist < WINDOW)
    ok = ok & ((lax.axis_index(SP) > 0) | (jnp.arange(2 * WINDOW)[None] >= WINDOW))
    s = jnp.where(ok, s, -1e30)
    sink = own_part(sink_logit, x, 2, 0)[None, :, None, None]
    top = jnp.maximum(jnp.max(s, -1, keepdims=True), sink)
    e = jnp.exp(s - top)
    den = jnp.sum(e, -1, keepdims=True) + jnp.exp(sink - top)
    att = jnp.einsum(
        "shqk,skd->sqhd",
        (e / den).astype(jnp.bfloat16),
        band[..., 64:],
        preferred_element_type=jnp.float32,
    ).astype(jnp.bfloat16)
    gla_out = local_out + jnp.einsum("snid,snde->snie", q_dec, entering, precision=HIGH)
    hidden = rms_rows(gla_out, head_gain).astype(jnp.bfloat16).reshape(-1, VALUE_DIM)
    hidden = jnp.concatenate([hidden, att.reshape(-1, 128)], axis=1)
    total = jnp.einsum("rk,nk->rn", hidden, w_out, preferred_element_type=jnp.float32)
    total = total.astype(jnp.bfloat16).reshape(8, -1, total.shape[1])
    arrived = lax.all_to_all(total, GROUP, split_axis=0, concat_axis=0, tiled=True)
    return arrived.astype(jnp.float32).sum(axis=0).astype(jnp.bfloat16)[None]


def solution(mesh):
    split = Mesh(
        mesh.devices.reshape(8, 8, mesh.shape["fs"], mesh.shape["tp"]), ("sp_0", "sp_1", "fs", "tp")
    )
    return jax.shard_map(
        per_device,
        mesh=split,
        in_specs=(
            P("fs", SP_TP, None),
            P(),
            P(SP, "tp"),
            P(SP, "tp"),
            P(SP, "tp"),
            P(SP, None),
            P(None, "tp"),
            P("tp"),
            P(),
            P(SP, "tp"),
            P(SP, "tp"),
            P(SP, "tp"),
            P("tp"),
            P("tp", SP),
            P("tp", SP),
        ),
        out_specs=P("fs", SP_TP, None),
        check_vma=False,
    )
```

profile of v0, /device:TPU:1, one launch (start us, length us, event | category | flops | bytes accessed | tf_op | source)
XLA Modules:
  0.0 351.1 jit_solution(2613073268380290763)
XLA Ops:
  6.5 0.0 copy-start
  6.5 0.0 all-gather.13.cloned.1.call-start
  6.5 0.7 all-gather.13.cloned.1.call-update
  7.3 0.0 all-gather.9.cloned.1.call-start
  7.3 0.8 constant_dynamic-slice_fusion.2
  8.1 0.8 constant_dynamic-slice_fusion.6
  8.9 0.7 constant_dynamic-slice_fusion.4
  9.6 1.4 concatenate.18
  11.0 0.0 all-gather.9.cloned.1.call-update
  11.1 0.0 all-gather.15.cloned.1.call-start
  11.1 0.8 dynamic_slice.40
  11.9 34.1 %all-gather.13.cloned.1.call-done = bf16[1,512,2048]{2,1,0:T(8,128)(2,1)} async-done(((bf16[1,64,2048]{2,1,0:T(8,128)(2,1)}), bf16[1,512,2048]{2,1,0:T(8,128)(2,1)}) %all-gather.13.cloned.1.call-update) | async-done | bytes 2097168 | tf_op jit(solution)/shard_map/all_gather | solution.py:69
  46.0 2.2 fusion
  48.2 81.3 %all-gather.9.cloned.1.call-done = bf16[2048,544]{1,0:T(8,128)(2,1)} async-done(((bf16[32,544]{1,0:T(8,128)(2,1)}), bf16[2048,544]{1,0:T(8,128)(2,1)}) %all-gather.9.cloned.1.call-update) | async-done | bytes 2228240 | tf_op jit(solution)/shard_map/all_gather | solution.py:82
  129.5 3.2 fusion.10
  132.8 0.0 copy-start.3
  132.8 0.8 copy-done.3
  133.6 0.4 fusion.28
  133.9 0.1 copy.215
  134.1 0.2 reduce_window_sum.11
  134.3 0.1 copy.197
  134.5 0.1 copy.216
  134.6 0.1 copy.201
  134.7 0.4 fusion.20
  135.1 0.1 fusion.41
  135.2 0.0 copy-start.6
  135.3 0.7 pad_maximum_fusion
  136.0 0.0 all-gather.15.cloned.1.call-update
  136.0 0.0 all-gather.17.cloned.1.call-start
  136.1 40.0 %all-gather.15.cloned.1.call-done = f32[32,64,129]{2,1,0:T(8,128)} async-done(((f32[4,64,129]{2,1,0:T(8,128)}), f32[32,64,129]{2,1,0:T(8,128)}) %all-gather.15.cloned.1.call-update) | async-done | bytes 1056784 | tf_op jit(solution)/shard_map/all_gather | solution.py:42
  176.1 1.6 slice_reduce_fusion.7
  177.7 1.6 bitcast_add_fusion.9
  179.4 0.7 pad_maximum_fusion.1
  180.1 0.0 all-gather.17.cloned.1.call-update
  180.1 0.0 all-gather.11.cloned.1.call-start
  180.2 0.7 constant_dynamic-slice_fusion
  180.9 0.6 maximum_bitcast_fusion
  181.5 0.0 all-gather.11.cloned.1.call-update
  181.6 0.1 fusion.55
  181.7 0.0 copy-done.6
  181.7 0.1 dynamic_slice.41
  181.8 0.9 convert_multiply_fusion.2
  182.6 0.1 copy.214
  182.8 2.7 collective-permute-start
  185.5 0.6 convolution_select_fusion
  186.1 0.3 fusion.64
  186.4 1.0 collective-permute-done
  187.5 0.4 fusion.63
  187.9 0.1 broadcast_maximum_fusion
  187.9 0.2 fusion.15
  188.1 0.1 exponential_add_fusion
  188.2 0.3 fusion.13
  188.5 0.1 copy.208
  188.6 34.4 %all-gather.17.cloned.1.call-done = f32[32,64,129]{2,1,0:T(8,128)} async-done(((f32[4,64,129]{2,1,0:T(8,128)}), f32[32,64,129]{2,1,0:T(8,128)}) %all-gather.17.cloned.1.call-update) | async-done | bytes 1056784 | tf_op jit(solution)/shard_map/all_gather | solution.py:42
  223.1 1.6 slice_reduce_fusion.6
  224.7 0.0 copy-start.4
  224.7 2.0 bitcast_add_fusion
  226.7 0.5 multiply_reduce_fusion
  227.3 0.1 multiply_convert_fusion
  227.4 0.1 copy.209
  227.5 78.2 %all-gather.11.cloned.1.call-done = bf16[2048,256]{1,0:T(8,128)(2,1)} async-done(((bf16[32,256]{1,0:T(8,128)(2,1)}), bf16[2048,256]{1,0:T(8,128)(2,1)}) %all-gather.11.cloned.1.call-update) | async-done | bytes 1048592 | tf_op jit(solution)/shard_map/all_gather | solution.py:86
  305.7 2.0 convolution_convert_fusion
  307.7 35.7 %all_to_all.5 = bf16[8,64,2048]{2,1,0:T(8,128)(2,1)S(1)} all-to-all(bf16[8,64,2048]{2,1,0:T(8,128)(2,1)S(1)} %bitcast.222), channel_id=1, replica_groups=mesh['sp_0'=8,'sp_1'=8,'fs'=4,'tp'=2] {'fs','tp'}, dimensions={0} | all-to-all | bytes 4194304 | tf_op jit(solution)/shard_map/all_to_all | solution.py:142
  343.4 1.1 reduce_sum.42
  (24 shorter events, 0.3 us)
Async XLA Ops:
  6.5 127.0 %copy-start = (bf16[32,256]{1,0:T(8,128)(2,1)S(1)}, bf16[32,256]{1,0:T(8,128)(2,1)}, u32[]{:S(2)}) copy-start(bf16[32,256]{1,0:T(8,128)(2,1)} %param.21) | copy-start | bytes 49156
  6.5 123.0 %copy-start.5 = (f32[2048]{0:T(1024)S(1)}, f32[2048]{0:T(1024)}, u32[]{:S(2)}) copy-start(f32[2048]{0:T(1024)} %param.16) | copy-start | bytes 24580
  6.5 39.5 %all-gather.13.cloned.1.call-start = ((), (), s32[]{:S(2)}) async-start(), calls=%async_computation.3 | async-start | bytes 2359296 | tf_op jit(solution)/shard_map/all_gather | solution.py:69
  7.3 122.2 %all-gather.9.cloned.1.call-start = ((), (), s32[]{:S(2)}) async-start(), calls=%async_computation.1 | async-start | bytes 2662400 | tf_op jit(solution)/shard_map/all_gather | solution.py:82
  11.1 165.0 %all-gather.15.cloned.1.call-start = ((), (), s32[]{:S(2)}) async-start(), calls=%async_computation.4 | async-start | bytes 2359296 | tf_op jit(solution)/shard_map/all_gather | solution.py:42
  46.0 83.5 %copy-start.2 = (bf16[1,512,2048]{2,1,0:T(8,128)(2,1)S(1)}, bf16[1,512,2048]{2,1,0:T(8,128)(2,1)}, u32[]{:S(2)}) copy-start(bf16[1,512,2048]{2,1,0:T(8,128)(2,1)} %all-gather.13.cloned.1.call-done) | copy-start | bytes 6291460
  132.8 0.8 copy-start.3
  135.2 46.5 %copy-start.6 = (f32[8]{0:T(128)S(1)}, f32[8]{0:T(128)}, u32[]{:S(2)}) copy-start(f32[8]{0:T(128)} %param.27) | copy-start | bytes 100
  136.0 87.1 %all-gather.17.cloned.1.call-start = ((), (), s32[]{:S(2)}) async-start(), calls=%async_computation.5 | async-start | bytes 2359296 | tf_op jit(solution)/shard_map/all_gather | solution.py:42
  180.1 125.6 %all-gather.11.cloned.1.call-start = ((), (), s32[]{:S(2)}) async-start(), calls=%async_computation.2 | async-start | bytes 1064960 | tf_op jit(solution)/shard_map/all_gather | solution.py:86
  182.8 4.6 %collective-permute-start = (bf16[4,128,128]{1,2,0:T(8,128)(2,1)S(1)}, bf16[4,128,128]{1,2,0:T(8,128)(2,1)S(1)}, u32[]{:S(2)}, u32[]{:S(2)}) collective-permute-start(bf16[4,128,128]{1,2,0:T(8,128)(2,1)S(1)} %bitcast.238), channel_id=1, source_target_pairs={{0,8},{8,16},{16,24},{24,32},{32,40},{40,48},{48,56},{56,64},{64,7... | collective-permute-start | bytes 393224 | tf_op jit(solution)/shard_map/ppermute | solution.py:119
  188.2 36.6 %copy-start.1 = (f32[32,64,129]{2,1,0:T(8,128)S(1)}, f32[32,64,129]{2,1,0:T(8,128)}, u32[]{:S(2)}) copy-start(f32[32,64,129]{2,1,0:T(8,128)} %all-gather.15.cloned.1.call-done) | copy-start | bytes 3170308
  224.7 2.5 copy-start.4
Sparse Core Ops, SparseCore 0:
  9.5 36.4 all-gather.12
  49.0 80.4 all-gather.8
  136.1 39.8 all-gather.14
  180.2 42.7 all-gather.16
  226.0 79.6 all-gather.10
where the time goes:
time: 352 us; the launch traced here: 351 us
  waiting for transfers between devices  270 us (77%)
  blocking collectives  35.7 us (10%)
  other arithmetic  14.1 us (4%)
  between operations  13.5 us (4%)
  matrix products  8.02 us (2%)
  local copies, waits for them, and re-layouts  7.07 us (2%)
    all_gather x1, waiting for transfers between devices, per_device(): w_in = lax.all_gather(w_in, SP, axis=0, tiled=True)  81.3 us
    all_gather x1, waiting for transfers between devices, per_device(): w_out = lax.all_gather(w_out, SP, axis=0, tiled=True)  78.2 us
    all_gather x2, waiting for transfers between devices, carried_in(): pieces = lax.all_gather(both, axis)  74.4 us
    all_to_all x1, blocking collectives, per_device(): lax.all_to_all(total, GROUP, split_axis=0, concat_axis=0, tiled=True)  35.7 us
    all_gather x1, waiting for transfers between devices, per_device(): rows = lax.all_gather(tokens[0], GROUP, axis=0, tiled=True)  34.1 us
  transfers between devices with their start and end apart: 6, of which 6 were waited for; matrix products, arithmetic and copies ran while one was open for 4% of the time, Pallas kernels for 0%

commit v1 on v0

--- a/solution.py
+++ b/solution.py
@@ -66,7 +66,8 @@
     window_output_weight,
 ):
     x = lax.axis_index("fs")
-    rows = lax.all_gather(tokens[0], GROUP, axis=0, tiled=True)
+    copies = jnp.concatenate([tokens[0]] * lax.axis_size(GROUP), axis=0)
+    rows = lax.all_to_all(copies, GROUP, 0, 0, tiled=True)
     w_in = jnp.concatenate(
         [
             own_part(gla_query_weight, x, 64, 1),

time: 352 us -> 318 us (0.903)
  waiting for transfers between devices: 270 us -> 222 us
  starting transfers between devices: 2.84 us -> 13.2 us
  local copies, waits for them, and re-layouts: 7.07 us -> 11 us
    all_gather x1, waiting for transfers between devices: 81.3 us -> 41.6 us  [per_device(): w_in = lax.all_gather(w_in, SP, axis=0, tiled=True)]
    all_gather x1 -> x0, waiting for transfers between devices: 34.1 us -> none  [per_device(): rows = lax.all_gather(tokens[0], GROUP, axis=0, tiled=True)]
    all_to_all x0 -> x1, waiting for transfers between devices: none -> 26.1 us  [per_device(): rows = lax.all_to_all(copies, GROUP, 0, 0, tiled=True)]
    all_to_all x0 -> x1, starting transfers between devices: none -> 10.5 us  [per_device(): rows = lax.all_to_all(copies, GROUP, 0, 0, tiled=True)]
    unnamed x16 -> x25, local copies, waits for them, and re-layouts: 0.83 us -> 5.32 us
  transfers between devices with their start and end apart: 6 -> 6, of which waited for: 6 -> 6; matrix products, arithmetic and copies ran while one was open for 4% -> 5% of each run, Pallas kernels for 0% -> 0%
where the time goes in v1:
time: 318 us
  waiting for transfers between devices  222 us (70%)
  blocking collectives  35.7 us (11%)
  between operations  13.6 us (4%)
  other arithmetic  13.3 us (4%)
  starting transfers between devices  13.2 us (4%)
  local copies, waits for them, and re-layouts  11 us (3%)
  matrix products  8.55 us (3%)
    all_gather x1, waiting for transfers between devices, per_device(): w_out = lax.all_gather(w_out, SP, axis=0, tiled=True)  78.2 us
    all_gather x2, waiting for transfers between devices, carried_in(): pieces = lax.all_gather(both, axis)  75.4 us
    all_gather x1, waiting for transfers between devices, per_device(): w_in = lax.all_gather(w_in, SP, axis=0, tiled=True)  41.6 us
    all_to_all x1, blocking collectives, per_device(): lax.all_to_all(total, GROUP, split_axis=0, concat_axis=0, tiled=True)  35.7 us
    all_to_all x1, waiting for transfers between devices, per_device(): rows = lax.all_to_all(copies, GROUP, 0, 0, tiled=True)  26.1 us
    all_to_all x1, starting transfers between devices, per_device(): rows = lax.all_to_all(copies, GROUP, 0, 0, tiled=True)  10.5 us
  transfers between devices with their start and end apart: 6, of which 6 were waited for; matrix products, arithmetic and copies ran while one was open for 5% of the time, Pallas kernels for 0%

profile of v1, /device:TPU:1, one launch (start us, length us, event | category | flops | bytes accessed | tf_op | source)
XLA Modules:
  0.0 317.7 jit_solution(1539957181657134066)
XLA Ops:
  6.5 0.8 constant_dynamic-slice_fusion.6
  7.4 0.7 constant_dynamic-slice_fusion.4
  8.1 0.8 constant_dynamic-slice_fusion.2
  8.9 1.4 concatenate.22
  10.3 0.0 all-gather.7.cloned.1.call-update
  10.3 1.0 bitcast_dynamic-update-slice_fusion.6
  11.3 1.0 bitcast_dynamic-update-slice_fusion.5
  12.3 1.0 bitcast_dynamic-update-slice_fusion.4
  13.2 1.0 bitcast_dynamic-update-slice_fusion.3
  14.3 1.3 copy-done.3
  15.6 10.5 %all-to-all-start = ((bf16[8,64,2048]{2,1,0:T(8,128)(2,1)}), bf16[8,64,2048]{2,1,0:T(8,128)(2,1)S(1)}, u32[]{:S(2)}, u32[]{:S(2)}) async-start(bf16[8,64,2048]{2,1,0:T(8,128)(2,1)} %bitcast.234), calls=%async_computation | async-start | bytes 4194304 | tf_op jit(solution)/shard_map/all_to_all | solution.py:70
  26.1 0.0 all-gather.11.cloned.1.call-start
  26.1 0.1 dynamic_slice.40
  26.2 26.1 %all-to-all-done = bf16[8,64,2048]{2,1,0:T(8,128)(2,1)S(1)} async-done(((bf16[8,64,2048]{2,1,0:T(8,128)(2,1)}), bf16[8,64,2048]{2,1,0:T(8,128)(2,1)S(1)}, u32[]{:S(2)}, u32[]{:S(2)}) %all-to-all-start) | async-done | bytes 2097184 | tf_op jit(solution)/shard_map/all_to_all | solution.py:70
  52.3 0.5 multiply_reduce_fusion
  52.8 0.1 rsqrt.20
  52.9 1.9 fusion.1
  54.8 41.6 %all-gather.7.cloned.1.call-done = bf16[2048,544]{1,0:T(8,128)(2,1)} async-done(((bf16[32,544]{1,0:T(8,128)(2,1)}), bf16[2048,544]{1,0:T(8,128)(2,1)}) %all-gather.7.cloned.1.call-update) | async-done | bytes 2228240 | tf_op jit(solution)/shard_map/all_gather | solution.py:83
  96.3 3.8 %convolution_convert_fusion.1 = bf16[512,544]{0,1:T(8,128)(2,1)S(1)} fusion(bf16[512,2048]{1,0:T(8,128)(2,1)} %fusion.1, bf16[2048,544]{1,0:T(8,128)(2,1)} %all-gather.7.cloned.1.call-done), kind=kOutput, calls=%fused_computation.8 | convolution fusion | flops 1141129216 | bytes 4882432 | tf_op jit(solution)/shard_map/dot_general | solution.py:89
  100.2 0.1 copy.216
  100.3 0.4 fusion.19
  100.7 0.1 copy.215
  100.8 0.1 copy.197
  100.9 0.2 reduce_window_sum.11
  101.2 0.1 copy.201
  101.3 0.4 fusion.11
  101.8 0.1 fusion.32
  101.9 0.0 copy-start.7
  101.9 0.7 pad_maximum_fusion
  102.6 0.0 all-gather.11.cloned.1.call-update
  102.6 0.0 all-gather.13.cloned.1.call-start
  102.7 40.0 %all-gather.11.cloned.1.call-done = f32[32,64,129]{2,1,0:T(8,128)} async-done(((f32[4,64,129]{2,1,0:T(8,128)}), f32[32,64,129]{2,1,0:T(8,128)}) %all-gather.11.cloned.1.call-update) | async-done | bytes 1056784 | tf_op jit(solution)/shard_map/all_gather | solution.py:42
  142.7 1.6 slice_reduce_fusion.7
  144.3 1.6 bitcast_add_fusion.9
  146.0 0.7 pad_maximum_fusion.1
  146.7 0.0 all-gather.13.cloned.1.call-update
  146.7 0.0 all-gather.9.cloned.1.call-start
  146.8 0.7 constant_dynamic-slice_fusion
  147.5 0.6 maximum_bitcast_fusion
  148.1 0.0 all-gather.9.cloned.1.call-update
  148.2 0.1 fusion.46
  148.3 0.1 dynamic_slice.41
  148.5 2.7 collective-permute-start
  151.2 0.1 copy.214
  151.3 0.6 convolution_select_fusion
  151.9 0.3 fusion.55
  152.2 0.9 collective-permute-done
  153.2 0.4 fusion.54
  153.5 0.1 broadcast_maximum_fusion
  153.6 0.2 fusion.6
  153.8 0.1 exponential_add_fusion
  153.9 0.3 fusion.4
  154.2 0.1 copy.208
  154.3 35.4 %all-gather.13.cloned.1.call-done = f32[32,64,129]{2,1,0:T(8,128)} async-done(((f32[4,64,129]{2,1,0:T(8,128)}), f32[32,64,129]{2,1,0:T(8,128)}) %all-gather.13.cloned.1.call-update) | async-done | bytes 1056784 | tf_op jit(solution)/shard_map/all_gather | solution.py:42
  189.7 1.6 slice_reduce_fusion.6
  191.3 0.0 copy-start.5
  191.3 2.0 bitcast_add_fusion
  193.3 0.5 multiply_reduce_fusion.1
  193.9 0.1 multiply_convert_fusion
  194.0 0.1 copy.209
  194.1 78.2 %all-gather.9.cloned.1.call-done = bf16[2048,256]{1,0:T(8,128)(2,1)} async-done(((bf16[32,256]{1,0:T(8,128)(2,1)}), bf16[2048,256]{1,0:T(8,128)(2,1)}) %all-gather.9.cloned.1.call-update) | async-done | bytes 1048592 | tf_op jit(solution)/shard_map/all_gather | solution.py:87
  272.3 2.0 convolution_convert_fusion
  274.3 35.7 %all_to_all.14 = bf16[8,64,2048]{2,1,0:T(8,128)(2,1)S(1)} all-to-all(bf16[8,64,2048]{2,1,0:T(8,128)(2,1)S(1)} %bitcast.230), channel_id=1, replica_groups=mesh['sp_0'=8,'sp_1'=8,'fs'=4,'tp'=2] {'fs','tp'}, dimensions={0} | all-to-all | bytes 4194304 | tf_op jit(solution)/shard_map/all_to_all | solution.py:143
  310.1 1.1 reduce_sum.42
  (35 shorter events, 0.4 us)
Async XLA Ops:
  6.5 93.8 %copy-start = (bf16[32,256]{1,0:T(8,128)(2,1)S(1)}, bf16[32,256]{1,0:T(8,128)(2,1)}, u32[]{:S(2)}) copy-start(bf16[32,256]{1,0:T(8,128)(2,1)} %param.21) | copy-start | bytes 49156
  6.5 7.7 %copy-start.1 = (bf16[1,64,2048]{2,1,0:T(8,128)(2,1)S(1)}, bf16[1,64,2048]{2,1,0:T(8,128)(2,1)}, u32[]{:S(2)}) copy-start(bf16[1,64,2048]{2,1,0:T(8,128)(2,1)} %param.15) | copy-start | bytes 786436
  6.5 89.8 %all-gather.7.cloned.1.call-start = ((), (), s32[]{:S(2)}) async-start(), calls=%async_computation.2 | async-start | bytes 2662400 | tf_op jit(solution)/shard_map/all_gather | solution.py:83
  14.3 1.3 copy-start.3
  15.6 10.5 %copy-start.6 = (f32[256]{0:T(256)S(1)}, f32[256]{0:T(256)}, u32[]{:S(2)}) copy-start(f32[256]{0:T(256)} %param.22) | copy-start | bytes 3076
  15.6 36.7 %all-to-all-start = ((bf16[8,64,2048]{2,1,0:T(8,128)(2,1)}), bf16[8,64,2048]{2,1,0:T(8,128)(2,1)S(1)}, u32[]{:S(2)}, u32[]{:S(2)}) async-start(bf16[8,64,2048]{2,1,0:T(8,128)(2,1)} %bitcast.234), calls=%async_computation | async-start | bytes 4194304 | tf_op jit(solution)/shard_map/all_to_all | solution.py:70
  26.1 26.8 %copy-start.4 = (f32[2048]{0:T(1024)S(1)}, f32[2048]{0:T(1024)}, u32[]{:S(2)}) copy-start(f32[2048]{0:T(1024)} %param.16) | copy-start | bytes 24580
  26.1 116.6 %all-gather.11.cloned.1.call-start = ((), (), s32[]{:S(2)}) async-start(), calls=%async_computation.4 | async-start | bytes 2359296 | tf_op jit(solution)/shard_map/all_gather | solution.py:42
  101.9 46.4 %copy-start.7 = (f32[8]{0:T(128)S(1)}, f32[8]{0:T(128)}, u32[]{:S(2)}) copy-start(f32[8]{0:T(128)} %param.27) | copy-start | bytes 100
  102.6 87.1 %all-gather.13.cloned.1.call-start = ((), (), s32[]{:S(2)}) async-start(), calls=%async_computation.5 | async-start | bytes 2359296 | tf_op jit(solution)/shard_map/all_gather | solution.py:42
  146.7 125.6 %all-gather.9.cloned.1.call-start = ((), (), s32[]{:S(2)}) async-start(), calls=%async_computation.3 | async-start | bytes 1064960 | tf_op jit(solution)/shard_map/all_gather | solution.py:87
  148.5 4.6 %collective-permute-start = (bf16[4,128,128]{1,2,0:T(8,128)(2,1)S(1)}, bf16[4,128,128]{1,2,0:T(8,128)(2,1)S(1)}, u32[]{:S(2)}, u32[]{:S(2)}) collective-permute-start(bf16[4,128,128]{1,2,0:T(8,128)(2,1)S(1)} %bitcast.247), channel_id=1, source_target_pairs={{0,8},{8,16},{16,24},{24,32},{32,40},{40,48},{48,56},{56,64},{64,7... | collective-permute-start | bytes 393224 | tf_op jit(solution)/shard_map/ppermute | solution.py:120
  153.9 37.5 %copy-start.2 = (f32[32,64,129]{2,1,0:T(8,128)S(1)}, f32[32,64,129]{2,1,0:T(8,128)}, u32[]{:S(2)}) copy-start(f32[32,64,129]{2,1,0:T(8,128)} %all-gather.11.cloned.1.call-done) | copy-start | bytes 3170308
  191.3 2.5 copy-start.5
Sparse Core Ops, SparseCore 0:
  10.4 85.8 all-gather.6
  102.7 39.8 all-gather.10
  146.8 42.7 all-gather.12
  192.6 79.6 all-gather.8
